TPU v7x, 512 devices: a whole 4x4x16 slice. The times are simulated.
512 devices in a mesh: kv: 64 (over z, y), tp: 8 (over x, core).
Axes of the slice: x: 4, y: 4, z: 16, core: 2. Of those that a mesh axis runs over, the one named last changes fastest.
Arguments:
- tokens: bfloat16 [256, 4096], P(None, 'kv')
- lengths: int32 [64], replicated, may hold values from 1 to 4, 112 in all
- memory: float32 [64, 16, 128, 128], P('kv', 'tp'), may hold values from -0.6 to 0.6
- norm_gain: float32 [4096], P('kv'), may hold values from 0.1 to 1.9
- w_query: bfloat16 [4096, 2048], P('kv', 'tp'), may hold values from -0.09375 to 0.09375
- w_key: bfloat16 [4096, 2048], P('kv', 'tp'), may hold values from -0.09375 to 0.09375
- w_value: bfloat16 [4096, 2048], P('kv', 'tp'), may hold values from -0.09375 to 0.09375
- w_outgate: bfloat16 [4096, 2048], P('kv', 'tp'), may hold values from -0.09375 to 0.09375
- w_alpha: bfloat16 [4096, 16], P('kv'), may hold values from -0.09375 to 0.09375
- w_beta: bfloat16 [4096, 16], P('kv'), may hold values from -0.09375 to 0.09375
- decay_log: float32 [16], P('tp'), may hold values from -4 to 0.5
- decay_bias: float32 [16], P('tp'), may hold values from -1 to 1
- head_gain: float32 [128], replicated, may hold values from 0.1 to 1.9
- w_output: bfloat16 [2048, 4096], P('tp', 'kv'), may hold values from -0.125 to 0.125
- mlp_gain: float32 [4096], P('kv'), may hold values from 0.1 to 1.9
- w_gate: bfloat16 [4096, 11264], P('kv', 'tp'), may hold values from -0.09375 to 0.09375
- w_up: bfloat16 [4096, 11264], P('kv', 'tp'), may hold values from -0.09375 to 0.09375
- w_down: bfloat16 [11264, 4096], P('tp', 'kv'), may hold values from -0.0546875 to 0.0546875
Outputs:
- layer_out: bfloat16 [256, 4096], P(None, 'kv')
- new_memory: float32 [64, 16, 128, 128], P('kv', 'tp')
Inputs may be any that keep to these rules, and one draw needn't show every extreme that they name: How many of a sequence's 4 slots hold live tokens; the live ones come first; the lengths add up to seven quarters of 64, rounded down.
All inputs are finite; a program needn't handle non-finite values.
Results may differ from a plain program's by a relative error of at most 0.012.
Values may be sent and summed in bfloat16 or wider, within the bound.
A program may use at most 64 MiB of HBM per device.

v0:
```python
import math
import jax
import jax.numpy as jnp
from jax import lax
from jax.sharding import Mesh
from jax.sharding import PartitionSpec as P

D = 4096
DK = 128
DV = 128
NEW = 4
KV = ("kv_0", "kv_1")
epsilon = 1e-06


def split_up(shard, dim, peers):
    before, after = (shard.shape[:dim], shard.shape[dim + 1 :])
    return jnp.moveaxis(shard.reshape(*before, peers, -1, *after), dim, 0)


def sent_and_summed(shard, axis, dim):
    parts = split_up(shard, dim, lax.axis_size(axis))
    arrived = lax.all_to_all(parts, axis, split_axis=0, concat_axis=0, tiled=True)
    return arrived.astype(jnp.float32).sum(axis=0)


def in_one_piece(arrays, axis, dim, along):
    widths = [math.prod(a.shape[along:]) for a in arrays]
    both = jnp.concatenate(
        [a.reshape(*a.shape[:along], w) for a, w in zip(arrays, widths)], axis=along
    )
    filled = sent_and_summed(both, axis, dim)
    parts = jnp.split(filled, [sum(widths[:k]) for k in range(1, len(widths))], axis=along)
    return tuple(
        (b.reshape(*filled.shape[:along], *a.shape[along:]) for a, b in zip(arrays, parts))
    )


def copy_for_each(shard, axis):
    peers = lax.axis_size(axis)
    return lax.all_to_all(
        jnp.broadcast_to(shard[None], (peers, *shard.shape)), axis, 0, 0, tiled=True
    )


def joined_along(parts, dim):
    parts = jnp.moveaxis(parts, 0, dim)
    dims = parts.shape
    return parts.reshape(*dims[:dim], dims[dim] * dims[dim + 1], *dims[dim + 2 :])


def collect(shard, axis, dim):
    parts = copy_for_each(shard, axis)
    return joined_along(parts, dim)


def of_everyone(shard, axis):
    return copy_for_each(shard, axis).sum(axis=0)


def gather_in_order(shard, axes, order):
    parts = shard[None]
    for k in order:
        parts = lax.all_gather(parts, axes[k], axis=0, tiled=True)
    carried = [lax.axis_size(axes[k]) for k in reversed(order)]
    parts = parts.reshape(*carried, *shard.shape)
    turned = sorted(range(len(order)), key=lambda place: order[len(order) - 1 - place])
    return parts.transpose(*turned, *range(len(order), parts.ndim)).reshape(-1, *shard.shape)


def gather_axes(shard, axes, order, dim):
    return joined_along(gather_in_order(shard, axes, order), dim)


def over_copies(shard, axis):
    everything = copy_for_each(shard, axis)
    return jnp.sum(everything.astype(jnp.float32), axis=0)


def unit_rows(values):
    return values * lax.rsqrt(jnp.sum(values * values, axis=-1, keepdims=True) + epsilon)


def advance(memory, queries, key_rows, value_rows, decays, betas):
    outputs = []
    for step in range(queries.shape[1]):
        memory = jnp.exp(decays[:, step])[:, :, None, None] * memory
        predicted = jnp.einsum(
            "shde,shd->she", memory, key_rows[:, step], precision=lax.Precision.HIGHEST
        )
        correction = betas[:, step][:, :, None] * (value_rows[:, step] - predicted)
        memory = memory + key_rows[:, step][:, :, :, None] * correction[:, :, None, :]
        outputs.append(
            jnp.einsum("shde,shd->she", memory, queries[:, step], precision=lax.Precision.HIGHEST)
        )
    return (memory, jnp.stack(outputs, axis=1))


def per_device(
    tokens,
    lengths,
    memory,
    norm_gain,
    w_query,
    w_key,
    w_value,
    w_outgate,
    w_alpha,
    w_beta,
    decay_log,
    decay_bias,
    head_gain,
    w_output,
    mlp_gain,
    w_gate,
    w_up,
    w_down,
):
    total_rows = tokens.shape[0]
    kv_count = lax.axis_size(KV)
    kv_place = lax.axis_index(KV)
    tp_place = lax.axis_index("tp")
    own_rows = total_rows // kv_count
    seq_dev = memory.shape[0]
    heads_dev = memory.shape[1]
    token_f = tokens.astype(jnp.float32)
    squares = jnp.sum(token_f * token_f, axis=1)
    scaled = (token_f * norm_gain).astype(jnp.bfloat16)
    part_query = jnp.dot(scaled, w_query, preferred_element_type=jnp.float32)
    part_key = jnp.dot(scaled, w_key, preferred_element_type=jnp.float32)
    part_value = jnp.dot(scaled, w_value, preferred_element_type=jnp.float32)
    part_gate = jnp.dot(scaled, w_outgate, preferred_element_type=jnp.float32)
    part_alpha = jnp.dot(scaled, w_alpha, preferred_element_type=jnp.float32)
    part_beta = jnp.dot(scaled, w_beta, preferred_element_type=jnp.float32)
    sum_query, sum_key, sum_value, sum_gate, sum_alpha, sum_beta, own_squares = in_one_piece(
        (
            part_query.astype(jnp.bfloat16),
            part_key.astype(jnp.bfloat16),
            part_value.astype(jnp.bfloat16),
            part_gate.astype(jnp.bfloat16),
            part_alpha.astype(jnp.bfloat16),
            part_beta.astype(jnp.bfloat16),
            squares.astype(jnp.bfloat16),
        ),
        KV,
        0,
        1,
    )
    rstd = lax.rsqrt(own_squares / D + epsilon)[:, None]
    queries = (sum_query * rstd).astype(jnp.bfloat16)
    key_rows = (sum_key * rstd).astype(jnp.bfloat16)
    value_rows = (sum_value * rstd).astype(jnp.bfloat16)
    outgate = (sum_gate * rstd).astype(jnp.bfloat16)
    alphas = lax.dynamic_slice_in_dim(sum_alpha * rstd, tp_place * heads_dev, heads_dev, 1)
    beta_pre = lax.dynamic_slice_in_dim(sum_beta * rstd, tp_place * heads_dev, heads_dev, 1)
    own_lengths = lax.dynamic_slice_in_dim(lengths, kv_place * seq_dev, seq_dev)
    live = jnp.arange(NEW, dtype=jnp.int32)[None, :] < own_lengths[:, None]
    query_h = unit_rows(queries.astype(jnp.float32).reshape(seq_dev, NEW, heads_dev, DK)) * DK ** (
        -0.5
    )
    key_h = unit_rows(key_rows.astype(jnp.float32).reshape(seq_dev, NEW, heads_dev, DK))
    value_h = value_rows.astype(jnp.float32).reshape(seq_dev, NEW, heads_dev, DV)
    decays = -jnp.exp(decay_log) * jax.nn.softplus(alphas + decay_bias)
    decays = jnp.where(live[:, :, None], decays.reshape(seq_dev, NEW, heads_dev), 0.0)
    betas = jnp.where(
        live[:, :, None], jax.nn.sigmoid(beta_pre).reshape(seq_dev, NEW, heads_dev), 0.0
    )
    new_memory, attended = advance(memory, query_h, key_h, value_h, decays, betas)
    attended = attended * lax.rsqrt(jnp.mean(attended * attended, axis=-1, keepdims=True) + epsilon)
    gate_h = outgate.astype(jnp.float32).reshape(seq_dev, NEW, heads_dev, DV)
    mixed = (
        (attended * head_gain * jax.nn.silu(gate_h))
        .astype(jnp.bfloat16)
        .reshape(own_rows, heads_dev * DV)
    )
    attn_terms = jnp.dot(collect(mixed, KV, 0), w_output, preferred_element_type=jnp.float32)
    attn_total = of_everyone(attn_terms, "tp")
    hidden = (token_f + attn_total).astype(jnp.bfloat16)
    hidden_f = hidden.astype(jnp.float32)
    hidden_squares = jnp.sum(hidden_f * hidden_f, axis=1)
    hscaled = (hidden_f * mlp_gain).astype(jnp.bfloat16)
    all_live = (jnp.arange(NEW, dtype=jnp.int32)[None, :] < lengths[:, None]).reshape(total_rows)
    part_gate_rows = jnp.dot(hscaled, w_gate, preferred_element_type=jnp.float32)
    part_up_rows = jnp.dot(hscaled, w_up, preferred_element_type=jnp.float32)
    gate_rows, up_rows, mlp_squares = in_one_piece(
        (
            part_gate_rows.astype(jnp.bfloat16),
            part_up_rows.astype(jnp.bfloat16),
            hidden_squares.astype(jnp.bfloat16),
        ),
        KV,
        0,
        1,
    )
    rstd2 = lax.rsqrt(mlp_squares / D + epsilon)[:, None]
    active = (jax.nn.silu(gate_rows * rstd2) * (up_rows * rstd2)).astype(jnp.bfloat16)
    feed_terms = jnp.dot(
        gather_axes(active, KV, (0, 1), 0), w_down, preferred_element_type=jnp.float32
    )
    feed_total = over_copies(feed_terms.astype(jnp.bfloat16), "tp").astype(jnp.float32)
    layer_out = jnp.where(all_live[:, None], hidden_f + feed_total, 0.0).astype(jnp.bfloat16)
    return (layer_out, new_memory)


def solution(mesh):
    torus = Mesh(mesh.devices.reshape(16, 4, mesh.shape["tp"]), ("kv_0", "kv_1", "tp"))
    placed = (
        P(None, KV),
        P(),
        P(KV, "tp", None, None),
        P(KV),
        P(KV, "tp"),
        P(KV, "tp"),
        P(KV, "tp"),
        P(KV, "tp"),
        P(KV, None),
        P(KV, None),
        P("tp"),
        P("tp"),
        P(),
        P("tp", KV),
        P(KV),
        P(KV, "tp"),
        P(KV, "tp"),
        P("tp", KV),
    )
    return jax.shard_map(
        per_device,
        mesh=torus,
        in_specs=placed,
        out_specs=(P(None, KV), P(KV, "tp", None, None)),
        check_vma=False,
    )
```

profile of v0, /device:TPU:1, one launch (start us, length us, event | category | flops | bytes accessed | tf_op | source)
XLA Modules:
  0.0 242.6 jit_solution(11514970106353623751)
XLA Ops:
  0.7 0.8 fusion.21
  1.5 1.1 convolution_convert_fusion.5
  2.6 1.1 convolution_convert_fusion.4
  3.8 1.1 convolution_convert_fusion.3
  4.9 1.1 convolution_convert_fusion.2
  6.1 0.2 convolution_convert_fusion.8
  6.4 0.2 convolution_convert_fusion.7
  6.7 0.2 convert_element_type.139
  7.0 2.5 %concatenate.42 = bf16[64,4,1057]{2,1,0:T(4,128)(2,1)} concatenate(bf16[64,4,256]{2,1,0:T(4,128)(2,1)S(1)} %concatenate.36, bf16[64,4,256]{2,1,0:T(4,128)(2,1)S(1)} %concatenate.37, bf16[64,4,256]{2,1,0:T(4,128)(2,1)S(1)} %concatenate.38, bf16[64,4,256]{2,1,0:T(4,128)(2,1)S(1)} %concatenate.39, bf16[64,4,16]{2,1,0:T(4,128)(2,1)S(1)} %bitcast.169, ...), dimensions={2} | concatenate | bytes 1082368 | tf_op jit(solution)/shard_map/concatenate | solution.py:29
  9.5 19.3 %all-to-all-start = ((bf16[64,4,1057]{2,1,0:T(4,128)(2,1)}), bf16[64,4,1057]{2,1,0:T(4,128)(2,1)S(1)}, u32[]{:S(2)}, u32[]{:S(2)}) async-start(bf16[64,4,1057]{2,1,0:T(4,128)(2,1)} %concatenate.42), calls=%async_computation | async-start | bytes 1179648 | tf_op jit(solution)/shard_map/all_to_all | solution.py:23
  28.8 0.6 dynamic_slice.9
  29.4 0.6 iota_compare_fusion.1
  30.1 31.9 %all-to-all-done = bf16[64,4,1057]{2,1,0:T(4,128)(2,1)S(1)} async-done(((bf16[64,4,1057]{2,1,0:T(4,128)(2,1)}), bf16[64,4,1057]{2,1,0:T(4,128)(2,1)S(1)}, u32[]{:S(2)}, u32[]{:S(2)}) %all-to-all-start) | async-done | bytes 541216 | tf_op jit(solution)/shard_map/all_to_all | solution.py:23
  62.0 0.3 convert_reduce_fusion.1
  62.3 0.2 fusion.68
  62.8 0.2 exponential_reduce_fusion.1
  63.3 0.2 slice_reduce_fusion
  63.8 0.3 fusion.14
  64.1 0.3 fusion.12
  64.4 0.3 fusion.10
  65.0 0.2 fusion.8
  65.2 0.3 fusion.6
  65.6 0.3 fusion.4
  65.9 0.3 fusion.2
  66.3 0.2 multiply_add_fusion
  66.5 0.2 fusion
  67.1 22.2 %all_to_all.25 = bf16[64,4,256]{2,1,0:T(4,128)(2,1)S(1)} all-to-all(bf16[64,4,256]{2,1,0:T(4,128)(2,1)S(1)} %broadcast_in_dim.32), channel_id=1, replica_groups=mesh['kv_0'=16,'kv_1'=4,'tp'=8] {'kv_0','kv_1'}, dimensions={0} | all-to-all | bytes 262144 | tf_op jit(solution)/shard_map/all_to_all | solution.py:41
  89.4 0.2 fusion.85
  89.6 17.0 %all_to_all.26 = f32[8,256,64]{1,2,0:T(8,128)S(1)} all-to-all(f32[8,256,64]{1,2,0:T(8,128)S(1)} %broadcast_in_dim.33), channel_id=1, replica_groups=mesh['kv_0'=16,'kv_1'=4,'tp'=8] {'tp'}, dimensions={0} | all-to-all | bytes 1048576 | tf_op jit(solution)/shard_map/all_to_all | solution.py:41
  106.7 0.4 convolution_convert_fusion.1
  107.2 0.2 concatenate.43
  107.4 0.2 copy-done.5
  107.6 0.4 convolution_convert_fusion
  108.0 0.2 concatenate.44
  108.2 0.2 convert_element_type.140
  108.4 0.7 pad_maximum_fusion
  109.1 74.8 %all_to_all.27 = bf16[64,4,2817]{2,1,0:T(4,128)(2,1)S(1)} all-to-all(bf16[64,4,2817]{2,1,0:T(4,128)(2,1)S(1)} %pad_maximum_fusion), channel_id=1, replica_groups=mesh['kv_0'=16,'kv_1'=4,'tp'=8] {'kv_0','kv_1'}, dimensions={0} | all-to-all | bytes 2884608 | tf_op jit(solution)/shard_map/all_to_all | solution.py:23
  183.9 0.6 convert_reduce_fusion
  184.8 22.4 %all-gather.1 = bf16[16,4,1408]{2,1,0:T(4,128)(2,1)S(1)} all-gather(bf16[1,4,1408]{2,1,0:T(4,128)(2,1)S(1)} %fusion.47), channel_id=2, replica_groups=mesh['kv_0'=16,'kv_1'=4,'tp'=8] {'kv_0'}, dimensions={0}, use_global_device_ids=true | all-gather | bytes 191488 | tf_op jit(solution)/shard_map/all_gather | solution.py:64
  207.1 10.5 %all_gather.7 = bf16[64,4,1408]{2,1,0:T(4,128)(2,1)S(1)} all-gather(bf16[16,4,1408]{2,1,0:T(4,128)(2,1)S(1)} %all-gather.1), channel_id=1, replica_groups=mesh['kv_0'=16,'kv_1'=4,'tp'=8] {'kv_1'}, dimensions={0}, use_global_device_ids=true | all-gather | bytes 901120 | tf_op jit(solution)/shard_map/all_gather | solution.py:64
  217.7 0.2 copy.78
  217.9 0.2 reshape_reshape.3
  218.1 0.5 copy-done.4
  218.6 0.3 convolution_convert_fusion.6
  219.0 0.7 broadcast_in_dim.35
  219.7 15.8 %all-to-all-start.4 = ((bf16[8,256,64]{1,2,0:T(8,128)(2,1)}), bf16[8,256,64]{1,2,0:T(8,128)(2,1)S(1)}, u32[]{:S(2)}, u32[]{:S(2)}) async-start(bf16[8,256,64]{1,2,0:T(8,128)(2,1)} %broadcast_in_dim.35), calls=%async_computation.4 | async-start | bytes 524288 | tf_op jit(solution)/shard_map/all_to_all | solution.py:41
  235.6 6.3 %all-to-all-done.4 = bf16[8,256,64]{1,2,0:T(8,128)(2,1)S(1)} async-done(((bf16[8,256,64]{1,2,0:T(8,128)(2,1)}), bf16[8,256,64]{1,2,0:T(8,128)(2,1)S(1)}, u32[]{:S(2)}, u32[]{:S(2)}) %all-to-all-start.4) | async-done | bytes 262176 | tf_op jit(solution)/shard_map/all_to_all | solution.py:41
  242.0 0.6 fusion.26
  (71 shorter events, 2.7 us)
Async XLA Ops:
  0.6 106.1 %copy-start = (bf16[64,1408]{1,0:T(8,128)(2,1)S(1)}, bf16[64,1408]{1,0:T(8,128)(2,1)}, u32[]{:S(2)}) copy-start(bf16[64,1408]{1,0:T(8,128)(2,1)} %param.33) | copy-start | bytes 540676
  0.6 5.4 %copy-start.2 = (bf16[256,64]{0,1:T(8,128)(2,1)S(1)}, bf16[256,64]{0,1:T(8,128)(2,1)}, u32[]{:S(2)}) copy-start(bf16[256,64]{0,1:T(8,128)(2,1)} %param.18) | copy-start | bytes 98308
  0.7 5.4 %copy-start.7 = (f32[64]{0:T(128)S(1)}, f32[64]{0:T(128)}, u32[]{:S(2)}) copy-start(f32[64]{0:T(128)} %param.21) | copy-start | bytes 772
  0.7 5.4 %copy-start.11 = (bf16[64,16]{0,1:T(8,128)(2,1)S(1)}, bf16[64,16]{0,1:T(8,128)(2,1)}, u32[]{:S(2)}) copy-start(bf16[64,16]{0,1:T(8,128)(2,1)} %param.26) | copy-start | bytes 6148
  0.7 5.7 %copy-start.12 = (bf16[64,16]{0,1:T(8,128)(2,1)S(1)}, bf16[64,16]{0,1:T(8,128)(2,1)}, u32[]{:S(2)}) copy-start(bf16[64,16]{0,1:T(8,128)(2,1)} %param.27) | copy-start | bytes 6148
  6.0 22.8 %copy-start.10 = (s32[64]{0:T(128)S(1)}, s32[64]{0:T(128)}, u32[]{:S(2)}) copy-start(s32[64]{0:T(128)} %param.19) | copy-start | bytes 772
  6.0 24.1 %copy-start.13 = (f32[2]{0:T(128)S(1)}, f32[2]{0:T(128)}, u32[]{:S(2)}) copy-start(f32[2]{0:T(128)} %param.28) | copy-start | bytes 28
  6.0 24.1 %copy-start.14 = (f32[128]{0:T(128)S(1)}, f32[128]{0:T(128)}, u32[]{:S(2)}) copy-start(f32[128]{0:T(128)} %param.30) | copy-start | bytes 1540
  7.0 55.6 %copy-start.9 = (f32[2]{0:T(128)S(1)}, f32[2]{0:T(128)}, u32[]{:S(2)}) copy-start(f32[2]{0:T(128)} %param.29) | copy-start | bytes 28
  7.0 56.8 %copy-start.1 = (f32[1,2,128,128]{3,2,1,0:T(8,128)S(1)}, f32[1,2,128,128]{3,2,1,0:T(8,128)}, u32[]{:S(2)}) copy-start(f32[1,2,128,128]{3,2,1,0:T(8,128)} %param.20) | copy-start | bytes 393220
  9.5 52.5 %all-to-all-start = ((bf16[64,4,1057]{2,1,0:T(4,128)(2,1)}), bf16[64,4,1057]{2,1,0:T(4,128)(2,1)S(1)}, u32[]{:S(2)}, u32[]{:S(2)}) async-start(bf16[64,4,1057]{2,1,0:T(4,128)(2,1)} %concatenate.42), calls=%async_computation | async-start | bytes 1179648 | tf_op jit(solution)/shard_map/all_to_all | solution.py:23
  30.1 59.3 %copy-start.6 = (bf16[256,64]{0,1:T(8,128)(2,1)S(1)}, bf16[256,64]{0,1:T(8,128)(2,1)}, u32[]{:S(2)}) copy-start(bf16[256,64]{0,1:T(8,128)(2,1)} %param.31) | copy-start | bytes 98308
  66.5 40.1 %copy-start.3 = (f32[1,2,128,128]{3,2,1,0:T(8,128)}, f32[1,2,128,128]{3,2,1,0:T(8,128)S(1)}, u32[]{:S(2)}) copy-start(f32[1,2,128,128]{3,2,1,0:T(8,128)S(1)} %multiply_add_fusion) | copy-start | bytes 393220
  67.1 39.6 %copy-start.8 = (f32[64]{0:T(128)S(1)}, f32[64]{0:T(128)}, u32[]{:S(2)}) copy-start(f32[64]{0:T(128)} %param.32) | copy-start | bytes 772
  106.6 0.9 copy-start.5
  217.7 0.9 copy-start.4
  219.7 22.3 %all-to-all-start.4 = ((bf16[8,256,64]{1,2,0:T(8,128)(2,1)}), bf16[8,256,64]{1,2,0:T(8,128)(2,1)S(1)}, u32[]{:S(2)}, u32[]{:S(2)}) async-start(bf16[8,256,64]{1,2,0:T(8,128)(2,1)} %broadcast_in_dim.35), calls=%async_computation.4 | async-start | bytes 524288 | tf_op jit(solution)/shard_map/all_to_all | solution.py:41
where the time goes:
time: 243 us
  blocking collectives  147 us (60%)
  waiting for transfers between devices  38.2 us (16%)
  starting transfers between devices  35 us (14%)
  matrix products  8.38 us (3%)
  local copies, waits for them, and re-layouts  7.27 us (3%)
  other arithmetic  5.71 us (2%)
    all_to_all x1, blocking collectives, sent_and_summed(): lax.all_to_all(parts, axis, split_axis=0, concat_axis=0, tiled=True)  74.8 us
    all_to_all x2, blocking collectives, copy_for_each(): lax.all_to_all(jnp.broadcast_to(shard[None], (peers, *shard.shape)), axis...  39.2 us
    all_gather x2, blocking collectives, gather_in_order(): parts = lax.all_gather(parts, axes[k], axis=0, tiled=True)  32.9 us
    all_to_all x1, waiting for transfers between devices, sent_and_summed(): lax.all_to_all(parts, axis, split_axis=0, concat_axis=0, tiled=True)  31.9 us
    all_to_all x1, starting transfers between devices, sent_and_summed(): lax.all_to_all(parts, axis, split_axis=0, concat_axis=0, tiled=True)  19.3 us
    all_to_all x1, starting transfers between devices, copy_for_each(): lax.all_to_all(jnp.broadcast_to(shard[None], (peers, *shard.shape)), axis...  15.8 us
    all_to_all x1, waiting for transfers between devices, copy_for_each(): lax.all_to_all(jnp.broadcast_to(shard[None], (peers, *shard.shape)), axis...  6.3 us
  transfers between devices with their start and end apart: 2, of which 2 were waited for; matrix products, arithmetic and copies ran while one was open for 1% of the time, Pallas kernels for 0%

commit v1 on v0

--- a/solution.py
+++ b/solution.py
@@ -61,7 +61,9 @@
 def gather_in_order(shard, axes, order):
     parts = shard[None]
     for k in order:
-        parts = lax.all_gather(parts, axes[k], axis=0, tiled=True)
+        parts = jnp.concatenate(
+            lax.all_to_all(jnp.stack([parts] * lax.axis_size(axes[k])), axes[k], 0, 0), axis=0
+        )
     carried = [lax.axis_size(axes[k]) for k in reversed(order)]
     parts = parts.reshape(*carried, *shard.shape)
     turned = sorted(range(len(order)), key=lambda place: order[len(order) - 1 - place])

time: 243 us -> 234 us (0.963)
  starting transfers between devices: 35 us -> 29.1 us
  blocking collectives: 147 us -> 143 us
    all_gather x2 -> x0, blocking collectives: 32.9 us -> none  [gather_in_order(): parts = lax.all_gather(parts, axes[k], axis=0, tiled=True)]
    all_to_all x0 -> x2, blocking collectives: none -> 29.3 us  [gather_in_order(): lax.all_to_all(jnp.stack([parts] * lax.axis_size(axes[k])), axes[k], 0, 0)]
    all_to_all x1, starting transfers between devices: 15.8 us -> 9.86 us  [copy_for_each(): lax.all_to_all(jnp.broadcast_to(shard[None], (peers, *shard.shape)), axis...]
where the time goes in v1:
time: 234 us; the launch traced here: 233 us
  blocking collectives  143 us (61%)
  waiting for transfers between devices  38.2 us (16%)
  starting transfers between devices  29.1 us (12%)
  matrix products  8.38 us (4%)
  local copies, waits for them, and re-layouts  7.51 us (3%)
  other arithmetic  5.71 us (2%)
    all_to_all x1, blocking collectives, sent_and_summed(): lax.all_to_all(parts, axis, split_axis=0, concat_axis=0, tiled=True)  74.8 us
    all_to_all x2, blocking collectives, copy_for_each(): lax.all_to_all(jnp.broadcast_to(shard[None], (peers, *shard.shape)), axis...  39.2 us
    all_to_all x1, waiting for transfers between devices, sent_and_summed(): lax.all_to_all(parts, axis, split_axis=0, concat_axis=0, tiled=True)  31.9 us
    all_to_all x2, blocking collectives, gather_in_order(): lax.all_to_all(jnp.stack([parts] * lax.axis_size(axes[k])), axes[k], 0, 0)  29.3 us
    all_to_all x1, starting transfers between devices, sent_and_summed(): lax.all_to_all(parts, axis, split_axis=0, concat_axis=0, tiled=True)  19.3 us
    all_to_all x1, starting transfers between devices, copy_for_each(): lax.all_to_all(jnp.broadcast_to(shard[None], (peers, *shard.shape)), axis...  9.86 us
    all_to_all x1, waiting for transfers between devices, copy_for_each(): lax.all_to_all(jnp.broadcast_to(shard[None], (peers, *shard.shape)), axis...  6.3 us
  transfers between devices with their start and end apart: 2, of which 2 were waited for; matrix products, arithmetic and copies ran while one was open for 1% of the time, Pallas kernels for 0%

profile of v1, /device:TPU:1, one launch (start us, length us, event | category | flops | bytes accessed | tf_op | source)
XLA Modules:
  0.0 233.3 jit_solution(2478188476009651068)
XLA Ops:
  0.7 0.8 fusion.21
  1.5 1.1 convolution_convert_fusion.5
  2.6 1.1 convolution_convert_fusion.4
  3.8 1.1 convolution_convert_fusion.3
  4.9 1.1 convolution_convert_fusion.2
  6.1 0.2 convolution_convert_fusion.8
  6.4 0.2 convolution_convert_fusion.7
  6.7 0.2 convert_element_type.139
  7.0 2.5 %concatenate.42 = bf16[64,4,1057]{2,1,0:T(4,128)(2,1)} concatenate(bf16[64,4,256]{2,1,0:T(4,128)(2,1)S(1)} %concatenate.36, bf16[64,4,256]{2,1,0:T(4,128)(2,1)S(1)} %concatenate.37, bf16[64,4,256]{2,1,0:T(4,128)(2,1)S(1)} %concatenate.38, bf16[64,4,256]{2,1,0:T(4,128)(2,1)S(1)} %concatenate.39, bf16[64,4,16]{2,1,0:T(4,128)(2,1)S(1)} %bitcast.165, ...), dimensions={2} | concatenate | bytes 1082368 | tf_op jit(solution)/shard_map/concatenate | solution.py:29
  9.5 19.3 %all-to-all-start = ((bf16[64,4,1057]{2,1,0:T(4,128)(2,1)}), bf16[64,4,1057]{2,1,0:T(4,128)(2,1)S(1)}, u32[]{:S(2)}, u32[]{:S(2)}) async-start(bf16[64,4,1057]{2,1,0:T(4,128)(2,1)} %concatenate.42), calls=%async_computation | async-start | bytes 1179648 | tf_op jit(solution)/shard_map/all_to_all | solution.py:23
  28.8 0.6 dynamic_slice.9
  29.4 0.6 iota_compare_fusion.1
  30.1 31.9 %all-to-all-done = bf16[64,4,1057]{2,1,0:T(4,128)(2,1)S(1)} async-done(((bf16[64,4,1057]{2,1,0:T(4,128)(2,1)}), bf16[64,4,1057]{2,1,0:T(4,128)(2,1)S(1)}, u32[]{:S(2)}, u32[]{:S(2)}) %all-to-all-start) | async-done | bytes 541216 | tf_op jit(solution)/shard_map/all_to_all | solution.py:23
  62.0 0.3 convert_reduce_fusion.1
  62.3 0.2 fusion.67
  62.8 0.2 exponential_reduce_fusion.1
  63.3 0.2 slice_reduce_fusion
  63.8 0.3 fusion.14
  64.1 0.3 fusion.12
  64.4 0.3 fusion.10
  65.0 0.2 fusion.8
  65.2 0.3 fusion.6
  65.6 0.3 fusion.4
  65.9 0.3 fusion.2
  66.3 0.2 multiply_add_fusion
  66.5 0.2 fusion
  67.1 22.2 %all_to_all.35 = bf16[64,4,256]{2,1,0:T(4,128)(2,1)S(1)} all-to-all(bf16[64,4,256]{2,1,0:T(4,128)(2,1)S(1)} %broadcast_in_dim.30), channel_id=1, replica_groups=mesh['kv_0'=16,'kv_1'=4,'tp'=8] {'kv_0','kv_1'}, dimensions={0} | all-to-all | bytes 262144 | tf_op jit(solution)/shard_map/all_to_all | solution.py:41
  89.6 17.0 %all_to_all.36 = f32[8,256,64]{1,2,0:T(8,128)S(1)} all-to-all(f32[8,256,64]{1,2,0:T(8,128)S(1)} %broadcast_in_dim.31), channel_id=1, replica_groups=mesh['kv_0'=16,'kv_1'=4,'tp'=8] {'tp'}, dimensions={0} | all-to-all | bytes 1048576 | tf_op jit(solution)/shard_map/all_to_all | solution.py:41
  106.7 0.4 convolution_convert_fusion.1
  107.2 0.2 concatenate.43
  107.4 0.2 copy-done.5
  107.6 0.4 convolution_convert_fusion
  108.0 0.2 concatenate.44
  108.2 0.2 convert_element_type.140
  108.4 0.7 pad_maximum_fusion
  109.1 74.8 %all_to_all.37 = bf16[64,4,2817]{2,1,0:T(4,128)(2,1)S(1)} all-to-all(bf16[64,4,2817]{2,1,0:T(4,128)(2,1)S(1)} %pad_maximum_fusion), channel_id=1, replica_groups=mesh['kv_0'=16,'kv_1'=4,'tp'=8] {'kv_0','kv_1'}, dimensions={0} | all-to-all | bytes 2884608 | tf_op jit(solution)/shard_map/all_to_all | solution.py:23
  183.9 0.6 convert_reduce_fusion
  184.8 18.1 %all_to_all.38 = bf16[16,1,4,1408]{3,2,1,0:T(4,128)(2,1)S(1)} all-to-all(bf16[16,1,4,1408]{3,2,1,0:T(4,128)(2,1)S(1)} %stack.41), channel_id=1, replica_groups=mesh['kv_0'=16,'kv_1'=4,'tp'=8] {'kv_0'}, dimensions={0} | all-to-all | bytes 360448 | tf_op jit(solution)/shard_map/all_to_all | solution.py:65
  202.9 0.2 stack.42
  203.1 11.2 %all_to_all.39 = bf16[4,16,4,1408]{3,2,1,0:T(4,128)(2,1)S(1)} all-to-all(bf16[4,16,4,1408]{3,2,1,0:T(4,128)(2,1)S(1)} %stack.42), channel_id=1, replica_groups=mesh['kv_0'=16,'kv_1'=4,'tp'=8] {'kv_1'}, dimensions={0} | all-to-all | bytes 1441792 | tf_op jit(solution)/shard_map/all_to_all | solution.py:65
  214.3 0.2 copy.55
  214.6 0.2 reshape_reshape.3
  214.7 0.5 copy-done.4
  215.2 0.3 convolution_convert_fusion.6
  215.6 0.7 broadcast_in_dim.32
  216.3 9.9 %all-to-all-start.6 = ((bf16[8,256,64]{1,2,0:T(8,128)(2,1)}), bf16[8,256,64]{1,2,0:T(8,128)(2,1)S(1)}, u32[]{:S(2)}, u32[]{:S(2)}) async-start(bf16[8,256,64]{1,2,0:T(8,128)(2,1)} %broadcast_in_dim.32), calls=%async_computation.6 | async-start | bytes 524288 | tf_op jit(solution)/shard_map/all_to_all | solution.py:41
  226.4 6.3 %all-to-all-done.6 = bf16[8,256,64]{1,2,0:T(8,128)(2,1)S(1)} async-done(((bf16[8,256,64]{1,2,0:T(8,128)(2,1)}), bf16[8,256,64]{1,2,0:T(8,128)(2,1)S(1)}, u32[]{:S(2)}, u32[]{:S(2)}) %all-to-all-start.6) | async-done | bytes 262176 | tf_op jit(solution)/shard_map/all_to_all | solution.py:41
  232.7 0.6 fusion.26
  (73 shorter events, 2.9 us)
Async XLA Ops:
  0.6 106.1 %copy-start = (bf16[64,1408]{1,0:T(8,128)(2,1)S(1)}, bf16[64,1408]{1,0:T(8,128)(2,1)}, u32[]{:S(2)}) copy-start(bf16[64,1408]{1,0:T(8,128)(2,1)} %param.33) | copy-start | bytes 540676
  0.6 5.4 %copy-start.2 = (bf16[256,64]{0,1:T(8,128)(2,1)S(1)}, bf16[256,64]{0,1:T(8,128)(2,1)}, u32[]{:S(2)}) copy-start(bf16[256,64]{0,1:T(8,128)(2,1)} %param.18) | copy-start | bytes 98308
  0.7 5.4 %copy-start.7 = (f32[64]{0:T(128)S(1)}, f32[64]{0:T(128)}, u32[]{:S(2)}) copy-start(f32[64]{0:T(128)} %param.21) | copy-start | bytes 772
  0.7 5.4 %copy-start.11 = (bf16[64,16]{0,1:T(8,128)(2,1)S(1)}, bf16[64,16]{0,1:T(8,128)(2,1)}, u32[]{:S(2)}) copy-start(bf16[64,16]{0,1:T(8,128)(2,1)} %param.26) | copy-start | bytes 6148
  0.7 5.7 %copy-start.12 = (bf16[64,16]{0,1:T(8,128)(2,1)S(1)}, bf16[64,16]{0,1:T(8,128)(2,1)}, u32[]{:S(2)}) copy-start(bf16[64,16]{0,1:T(8,128)(2,1)} %param.27) | copy-start | bytes 6148
  6.0 22.8 %copy-start.10 = (s32[64]{0:T(128)S(1)}, s32[64]{0:T(128)}, u32[]{:S(2)}) copy-start(s32[64]{0:T(128)} %param.19) | copy-start | bytes 772
  6.0 24.1 %copy-start.13 = (f32[2]{0:T(128)S(1)}, f32[2]{0:T(128)}, u32[]{:S(2)}) copy-start(f32[2]{0:T(128)} %param.28) | copy-start | bytes 28
  6.0 24.1 %copy-start.14 = (f32[128]{0:T(128)S(1)}, f32[128]{0:T(128)}, u32[]{:S(2)}) copy-start(f32[128]{0:T(128)} %param.30) | copy-start | bytes 1540
  7.0 55.6 %copy-start.9 = (f32[2]{0:T(128)S(1)}, f32[2]{0:T(128)}, u32[]{:S(2)}) copy-start(f32[2]{0:T(128)} %param.29) | copy-start | bytes 28
  7.0 56.8 %copy-start.1 = (f32[1,2,128,128]{3,2,1,0:T(8,128)S(1)}, f32[1,2,128,128]{3,2,1,0:T(8,128)}, u32[]{:S(2)}) copy-start(f32[1,2,128,128]{3,2,1,0:T(8,128)} %param.20) | copy-start | bytes 393220
  9.5 52.5 %all-to-all-start = ((bf16[64,4,1057]{2,1,0:T(4,128)(2,1)}), bf16[64,4,1057]{2,1,0:T(4,128)(2,1)S(1)}, u32[]{:S(2)}, u32[]{:S(2)}) async-start(bf16[64,4,1057]{2,1,0:T(4,128)(2,1)} %concatenate.42), calls=%async_computation | async-start | bytes 1179648 | tf_op jit(solution)/shard_map/all_to_all | solution.py:23
  30.1 59.3 %copy-start.6 = (bf16[256,64]{0,1:T(8,128)(2,1)S(1)}, bf16[256,64]{0,1:T(8,128)(2,1)}, u32[]{:S(2)}) copy-start(bf16[256,64]{0,1:T(8,128)(2,1)} %param.31) | copy-start | bytes 98308
  66.5 40.1 %copy-start.3 = (f32[1,2,128,128]{3,2,1,0:T(8,128)}, f32[1,2,128,128]{3,2,1,0:T(8,128)S(1)}, u32[]{:S(2)}) copy-start(f32[1,2,128,128]{3,2,1,0:T(8,128)S(1)} %multiply_add_fusion) | copy-start | bytes 393220
  67.1 39.6 %copy-start.8 = (f32[64]{0:T(128)S(1)}, f32[64]{0:T(128)}, u32[]{:S(2)}) copy-start(f32[64]{0:T(128)} %param.32) | copy-start | bytes 772
  106.6 0.9 copy-start.5
  214.3 0.9 copy-start.4
  216.3 16.4 %all-to-all-start.6 = ((bf16[8,256,64]{1,2,0:T(8,128)(2,1)}), bf16[8,256,64]{1,2,0:T(8,128)(2,1)S(1)}, u32[]{:S(2)}, u32[]{:S(2)}) async-start(bf16[8,256,64]{1,2,0:T(8,128)(2,1)} %broadcast_in_dim.32), calls=%async_computation.6 | async-start | bytes 524288 | tf_op jit(solution)/shard_map/all_to_all | solution.py:41
